TPU v7x, 512 devices: a whole 4x4x16 slice. The times are simulated.
512 devices in a mesh: sp: 64 (over z, y), tp: 8 (over x, core).
Axes of the slice: x: 4, y: 4, z: 16, core: 2. Of those that a mesh axis runs over, the one named last changes fastest.
Arguments:
- residual_signal: bfloat16 [16384, 2048], P('sp'), may hold values from -6 to 6
- reading_probe_preactivations: bfloat16 [16384, 1024], P('sp', 'tp'), may hold values from -6 to 6
- keep_switch_preactivations: bfloat16 [16384, 1024], P('sp', 'tp'), may hold values from -5.5 to 5.5
- written_entries: bfloat16 [16384, 1024], P('sp', 'tp'), may hold values from -6 to 6
- emission_switch_preactivations: bfloat16 [16384, 1024], P('sp', 'tp'), may hold values from -6 to 6
- additional_shrink_amount: float32 [16384, 1024], P('sp', 'tp'), may hold values from -0.7 to 0
- complement_of_floor: float32 [1024], P('tp'), may hold values from 6.1035156e-06 to 0.1
- per_group_rescaler: float32 [128], replicated, may hold values from 0.1 to 1.9
- emission_linear_map: bfloat16 [1024, 2048], P('tp'), may hold values from -0.1875 to 0.1875
- channel_layer_rescaler: float32 [2048], replicated, may hold values from 0.1 to 1.9
- expanding_linear_map: bfloat16 [2048, 8192], P('sp', 'tp'), may hold values from -0.125 to 0.125
- contracting_linear_map: bfloat16 [2048, 8192], P('sp', 'tp'), may hold values from -0.0625 to 0.0625
Outputs:
- layer_out: bfloat16 [16384, 2048], P('sp')
All inputs are finite; a program needn't handle non-finite values.
Results may differ from a plain program's by a relative error of at most 0.006.
Values may be sent and summed in bfloat16 or wider, within the bound.
A program may use at most 64 MiB of HBM per device.

v0:
```python
import jax
import jax.numpy as jnp
from jax import lax
from jax.sharding import Mesh
from jax.sharding import PartitionSpec as P

HEAD = 128
BLOCK = 64
SP = ("sp_0", "sp_1")
norm_eps = 1e-06
HIGH_ACCURACY = lax.Precision.HIGHEST


def filled_with(shard, identity):
    return jax.tree.map(
        lambda a, e: jnp.broadcast_to(jnp.asarray(e, a.dtype), a.shape), shard, identity
    )


def gathered_once(shard, axis):
    leaves = jax.tree.leaves(shard)
    turns = sorted(range(len(leaves)), key=lambda k: -leaves[k].size)
    width = (1, *leaves[turns[0]].shape)[-1]
    lines = [
        jnp.pad(leaves[k].reshape(-1), (0, -leaves[k].size % width)).reshape(-1, width)
        for k in turns
    ]
    both, at, found = (lax.all_gather(jnp.concatenate(lines), axis), 0, {})
    for k, line in zip(turns, lines):
        piece = both[:, at : at + len(line)].reshape(len(both), -1)
        found[k] = piece[:, : leaves[k].size].reshape(-1, *leaves[k].shape)
        at += len(line)
    numbers = iter(range(len(leaves)))
    return jax.tree.map(lambda _: found[next(numbers)], shard)


def entering(shard, axes, combine, identity):
    before = start = filled_with(shard, identity)
    total = shard
    for axis in reversed(axes):
        peers, index = (lax.axis_size(axis), lax.axis_index(axis))
        pieces = gathered_once(total, axis)
        inside, total = (start, start)
        for k in range(peers):
            passed = k < index
            total = combine(total, jax.tree.map(lambda part: part[k], pieces))
            inside = jax.tree.map(lambda new, old: jnp.where(passed, new, old), total, inside)
        before = combine(inside, before)
    return before


def laid_out(blocks, dim):
    lengths = list(blocks.shape[1:])
    lengths[dim] *= blocks.shape[0]
    return jnp.moveaxis(blocks, 0, dim).reshape(lengths)


def copy_for_each(shard, axis):
    peers = lax.axis_size(axis)
    return lax.all_to_all(
        jnp.broadcast_to(shard[None], (peers, *shard.shape)), axis, 0, 0, tiled=True
    )


def gathered_copies(shard, axis, dim):
    return laid_out(copy_for_each(shard, axis), dim)


def in_one_piece(arrays, axis, dim, along):
    widths = [a.shape[along] for a in arrays]
    both = jnp.concatenate(arrays, axis=along)
    whole = lax.all_gather(both, axis, axis=dim, tiled=True)
    return tuple(jnp.split(whole, [sum(widths[:k]) for k in range(1, len(widths))], axis=along))


def cut_along(shard, dim, peers):
    lengths = shard.shape
    blocks = shard.reshape(*lengths[:dim], peers, lengths[dim] // peers, *lengths[dim + 1 :])
    return jnp.moveaxis(blocks, dim, 0)


def sum_at_owner(shard, axis, dim):
    blocks = cut_along(shard, dim, lax.axis_size(axis))
    arrived = lax.all_to_all(blocks, axis, split_axis=0, concat_axis=0, tiled=True)
    return arrived.astype(jnp.float32).sum(axis=0)


def block_step(state_matrix, inputs):
    query_block_rows, key_blk, logs_blk, value_block_rows = inputs
    cumulative_decay = jnp.cumsum(logs_blk, axis=1)
    carried_state = jnp.einsum(
        "rlb,rbz->rlz",
        query_block_rows * jnp.exp(cumulative_decay),
        state_matrix,
        precision=HIGH_ACCURACY,
    )
    spread = cumulative_decay[:, :, None, :] - cumulative_decay[:, None, :, :]
    places = jnp.arange(BLOCK)
    lower = places[:, None] >= places[None, :]
    decay = jnp.exp(jnp.where(lower[None, :, :, None], spread, -jnp.inf))
    scores = jnp.einsum(
        "htk,hsk,htsk->hts", query_block_rows, key_blk, decay, precision=HIGH_ACCURACY
    )
    result = carried_state + jnp.einsum(
        "hts,hsv->htv", scores, value_block_rows, precision=HIGH_ACCURACY
    )
    final_state = cumulative_decay[:, -1:, :]
    decayed_key_rows = key_blk * jnp.exp(final_state - cumulative_decay)
    state_matrix = jnp.exp(final_state[:, 0, :])[..., None] * state_matrix + jnp.einsum(
        "aux,auf->axf", decayed_key_rows, value_block_rows, precision=HIGH_ACCURACY
    )
    return (state_matrix, result)


def combine_carry(earlier, later):
    return (earlier[0] * later[0], later[0][..., None] * earlier[1] + later[1])


def body(
    residual_signal,
    reading_probe_preactivations,
    keep_switch_preactivations,
    written_entries,
    emission_switch_preactivations,
    additional_shrink_amount,
    complement_of_floor,
    per_group_rescaler,
    emission_linear_map,
    channel_layer_rescaler,
    expanding_linear_map,
    contracting_linear_map,
):
    positions = reading_probe_preactivations.shape[0]
    channels = reading_probe_preactivations.shape[1]
    local_heads = channels // HEAD
    count = positions // BLOCK
    query_act = jax.nn.silu(reading_probe_preactivations.astype(jnp.float32))
    logarithmic_keep_fraction = (
        jnp.logaddexp(
            jnp.log1p(-complement_of_floor),
            jnp.log(complement_of_floor)
            + jax.nn.log_sigmoid(keep_switch_preactivations.astype(jnp.float32)),
        )
        + additional_shrink_amount
    )
    key_part = -jnp.expm1(logarithmic_keep_fraction)
    value_part = written_entries.astype(jnp.float32)

    def to_blocks(values):
        return values.reshape(count, BLOCK, local_heads, HEAD).transpose(0, 2, 1, 3)

    start = jnp.zeros((local_heads, HEAD, HEAD), jnp.float32)
    state_end, outputs = lax.scan(
        block_step,
        start,
        (
            to_blocks(query_act),
            to_blocks(key_part),
            to_blocks(logarithmic_keep_fraction),
            to_blocks(value_part),
        ),
    )
    within_block_output = outputs.transpose(0, 2, 1, 3).reshape(positions, local_heads, HEAD)
    running = jnp.cumsum(logarithmic_keep_fraction, axis=0)
    decay_total = jnp.exp(running[-1]).reshape(local_heads, HEAD)
    identity = (
        jnp.ones((local_heads, HEAD), jnp.float32),
        jnp.zeros((local_heads, HEAD, HEAD), jnp.float32),
    )
    prior_state = entering((decay_total, state_end), SP, combine_carry, identity)
    weighted_scores = (query_act * jnp.exp(running)).reshape(positions, local_heads, HEAD)
    recurrent_output = within_block_output + jnp.einsum(
        "pnm,nmx->pnx", weighted_scores, prior_state[1], precision=HIGH_ACCURACY
    )
    scaled = (
        recurrent_output
        * lax.rsqrt(
            jnp.mean(recurrent_output * recurrent_output, axis=-1, keepdims=True) + norm_eps
        )
        * per_group_rescaler
    )
    gated = scaled * jax.nn.silu(emission_switch_preactivations.astype(jnp.float32)).reshape(
        positions, local_heads, HEAD
    )
    mixed_heads = gated.reshape(positions, channels).astype(jnp.bfloat16)
    all_heads = gathered_copies(mixed_heads, "tp", 1)
    full_out = lax.all_gather(emission_linear_map, "tp", axis=0, tiled=True)
    projected = jnp.dot(all_heads, full_out, preferred_element_type=jnp.float32)
    after_mix = residual_signal.astype(jnp.float32) + projected
    normed = (
        after_mix
        * lax.rsqrt(jnp.mean(after_mix * after_mix, axis=-1, keepdims=True) + norm_eps)
        * channel_layer_rescaler
    ).astype(jnp.bfloat16)
    up_whole, down_whole = in_one_piece((expanding_linear_map, contracting_linear_map), SP, 0, 1)
    upward = jnp.dot(normed, up_whole, preferred_element_type=jnp.float32)
    hidden = jnp.square(jax.nn.relu(upward)).astype(jnp.bfloat16)
    share = positions // lax.axis_size("tp")
    downward = sum_at_owner(
        lax.dot_general(
            hidden, down_whole, (((1,), (1,)), ((), ())), preferred_element_type=jnp.float32
        ).astype(jnp.bfloat16),
        "tp",
        0,
    )
    own_start = lax.axis_index("tp") * share
    own_mix = lax.dynamic_slice_in_dim(after_mix, own_start, share, 0)
    finished = (own_mix + downward).astype(jnp.bfloat16)
    return gathered_copies(finished, "tp", 0)


def solution(mesh):
    finer = Mesh(mesh.devices.reshape(16, 4, mesh.shape["tp"]), ("sp_0", "sp_1", "tp"))
    return jax.shard_map(
        body,
        mesh=finer,
        in_specs=(
            P(SP, None),
            P(SP, "tp"),
            P(SP, "tp"),
            P(SP, "tp"),
            P(SP, "tp"),
            P(SP, "tp"),
            P("tp"),
            P(),
            P("tp", None),
            P(),
            P(SP, "tp"),
            P(SP, "tp"),
        ),
        out_specs=P(SP, None),
        check_vma=False,
    )
```

profile of v0, /device:TPU:1, one launch (start us, length us, event | category | flops | bytes accessed | tf_op | source)
XLA Modules:
  0.0 363.2 jit_solution(13176499211492240413)
XLA Ops:
  6.5 0.7 negate_log-plus-one_fusion
  7.2 1.1 exponential-minus-one_negate_fusion
  8.9 1.0 copy.41
  10.1 13.1 %while.13 = (s32[]{:T(128)}, f32[1,128,128]{2,1,0:T(8,128)S(1)}, f32[4,1,64,128]{3,2,1,0:T(8,128)S(1)}, f32[4,1,64,128]{3,2,1,0:T(8,128)S(1)}, f32[4,1,64,128]{3...) while((s32[]{:T(128)}, f32[1,128,128]{2,1,0:T(8,128)S(1)}, ...), condition=%wide.region_2.3_spmd.clone, body=%wide.region_0.2_spmd.clone.sunk | while | flops 34693120 | bytes 5108864 | solution.py:153
  10.8 1.7 fusion.174
  14.1 1.7 fusion.174
  17.4 1.7 fusion.174
  20.6 1.7 fusion.174
  23.2 10.7 %all-gather.2 = f32[4,129,128]{2,1,0:T(8,128)S(1)} all-gather(f32[1,129,128]{2,1,0:T(8,128)S(1)} %maximum_bitcast_fusion), channel_id=2, replica_groups=mesh['sp_0'=16,'sp_1'=4,'tp'=8] {'sp_1'}, dimensions={0}, use_global_device_ids=true | all-gather | bytes 330240 | tf_op jit(solution)/shard_map/all_gather | solution.py:28
  34.1 0.6 maximum_bitcast_fusion.1
  34.8 0.7 all-gather.8.cloned.1.call-update
  35.6 0.7 pad_maximum_fusion
  36.5 65.5 %all-gather.12.cloned.1.call-done = f32[16,129,128]{2,1,0:T(8,128)} async-done(((f32[1,129,128]{2,1,0:T(8,128)}), f32[16,129,128]{2,1,0:T(8,128)}) %all-gather.12.cloned.1.call-update) | async-done | bytes 1056784 | tf_op jit(solution)/shard_map/all_gather | solution.py:28
  102.1 0.8 slice_bitcast_fusion.16
  102.8 2.1 multiply_reduce_fusion.1
  105.1 24.3 %all_to_all.15 = bf16[8,256,128]{1,2,0:T(8,128)(2,1)S(1)} all-to-all(bf16[8,256,128]{1,2,0:T(8,128)(2,1)S(1)} %broadcast_in_dim.32), channel_id=1, replica_groups=mesh['sp_0'=16,'sp_1'=4,'tp'=8] {'tp'}, dimensions={0} | all-to-all | bytes 1048576 | tf_op jit(solution)/shard_map/all_to_all | solution.py:60
  129.4 22.2 %all-gather.8.cloned.1.call-done = bf16[1024,2048]{1,0:T(8,128)(2,1)} async-done(((bf16[128,2048]{1,0:T(8,128)(2,1)}), bf16[1024,2048]{1,0:T(8,128)(2,1)}) %all-gather.8.cloned.1.call-update) | async-done | bytes 4194320 | tf_op jit(solution)/shard_map/all_gather | solution.py:187
  151.7 3.9 %multiply_reduce_fusion = (f32[256]{0:T(256)S(1)}, f32[256,2048]{1,0:T(8,128)S(1)}) fusion(bf16[256,1024]{0,1:T(8,128)(2,1)S(1)} %bitcast.218, bf16[1024,2048]{1,0:T(8,128)(2,1)} %all-gather.8.cloned.1.call-done, bf16[256,2048]{1,0:T(8,128)(2,1)} %param.14), kind=kOutput, calls=%fused_computation.45 | convolution fusion | flops 1075838720 | bytes 7865344 | tf_op jit(solution)/shard_map/dot_general | solution.py:188
  155.5 147.1 %all-gather.10.cloned.1.call-done = bf16[2048,2048]{1,0:T(8,128)(2,1)} async-done(((bf16[32,2048]{1,0:T(8,128)(2,1)}), bf16[2048,2048]{1,0:T(8,128)(2,1)}) %all-gather.10.cloned.1.call-update) | async-done | bytes 8388624 | tf_op jit(solution)/shard_map/all_gather | solution.py:72
  302.7 6.8 %fusion.32 = bf16[256,2048]{1,0:T(8,128)(2,1)} fusion(bf16[2048,2048]{1,0:T(8,128)(2,1)} %all-gather.10.cloned.1.call-done, f32[256,2048]{1,0:T(8,128)S(1)} %get-tuple-element.142, f32[2048]{0:T(1024)S(1)} %copy-done.5, f32[256]{0:T(256)S(1)} %add_rsqrt_fusion), kind=kOutput, calls=%fused_computation.42 | convolution fusion | flops 2150367232 | bytes 11543552 | tf_op jit(solution)/shard_map/dot_general | solution.py:200
  309.5 12.7 %all-to-all-start.1 = ((bf16[8,32,2048]{2,1,0:T(8,128)(2,1)}), bf16[8,32,2048]{2,1,0:T(8,128)(2,1)S(1)}, u32[]{:S(2)}, u32[]{:S(2)}) async-start(bf16[8,32,2048]{2,1,0:T(8,128)(2,1)} %bitcast.223), calls=%async_computation.1 | async-start | bytes 2097152 | tf_op jit(solution)/shard_map/all_to_all | solution.py:84
  322.2 15.0 %all-to-all-done.1 = bf16[8,32,2048]{2,1,0:T(8,128)(2,1)S(1)} async-done(((bf16[8,32,2048]{2,1,0:T(8,128)(2,1)}), bf16[8,32,2048]{2,1,0:T(8,128)(2,1)S(1)}, u32[]{:S(2)}, u32[]{:S(2)}) %all-to-all-start.1) | async-done | bytes 1048608 | tf_op jit(solution)/shard_map/all_to_all | solution.py:84
  337.4 18.3 %all_to_all.16 = bf16[8,32,2048]{2,1,0:T(8,128)(2,1)S(1)} all-to-all(bf16[8,32,2048]{2,1,0:T(8,128)(2,1)S(1)} %broadcast_in_dim.33), channel_id=1, replica_groups=mesh['sp_0'=16,'sp_1'=4,'tp'=8] {'tp'}, dimensions={0} | all-to-all | bytes 2097152 | tf_op jit(solution)/shard_map/all_to_all | solution.py:60
  355.7 1.0 copy.80
  (86 shorter events, 7.5 us)
Async XLA Ops:
  6.5 3.5 copy-start
  6.5 95.5 %all-gather.12.cloned.1.call-start = ((), (), s32[]{:S(2)}) async-start(), calls=%async_computation.5 | async-start | bytes 1183744 | tf_op jit(solution)/shard_map/all_gather | solution.py:28
  10.0 25.5 %copy-start.2 = (bf16[32,1024]{1,0:T(8,128)(2,1)S(1)}, bf16[32,1024]{1,0:T(8,128)(2,1)}, u32[]{:S(2)}) copy-start(bf16[32,1024]{1,0:T(8,128)(2,1)} %param.25) | copy-start | bytes 196612
  10.1 25.5 %copy-start.3 = (bf16[32,1024]{1,0:T(8,128)(2,1)S(1)}, bf16[32,1024]{1,0:T(8,128)(2,1)}, u32[]{:S(2)}) copy-start(bf16[32,1024]{1,0:T(8,128)(2,1)} %param.24) | copy-start | bytes 196612
  23.1 13.3 %copy-start.1 = (bf16[256,128]{1,0:T(8,128)(2,1)S(1)}, bf16[256,128]{1,0:T(8,128)(2,1)}, u32[]{:S(2)}) copy-start(bf16[256,128]{1,0:T(8,128)(2,1)} %param.18) | copy-start | bytes 196612
  34.7 70.2 %copy-start.4 = (f32[128]{0:T(128)S(1)}, f32[128]{0:T(128)}, u32[]{:S(2)}) copy-start(f32[128]{0:T(128)} %param.21) | copy-start | bytes 1540
  34.7 116.9 %all-gather.8.cloned.1.call-start = ((), (), s32[]{:S(2)}) async-start(), calls=%async_computation.3 | async-start | bytes 4718592 | tf_op jit(solution)/shard_map/all_gather | solution.py:187
  35.5 267.2 %all-gather.10.cloned.1.call-start = ((), (), s32[]{:S(2)}) async-start(), calls=%async_computation.4 | async-start | bytes 8519680 | tf_op jit(solution)/shard_map/all_gather | solution.py:72
  151.7 151.0 %copy-start.5 = (f32[2048]{0:T(1024)S(1)}, f32[2048]{0:T(1024)}, u32[]{:S(2)}) copy-start(f32[2048]{0:T(1024)} %param.23) | copy-start | bytes 24580
  309.5 27.6 %all-to-all-start.1 = ((bf16[8,32,2048]{2,1,0:T(8,128)(2,1)}), bf16[8,32,2048]{2,1,0:T(8,128)(2,1)S(1)}, u32[]{:S(2)}, u32[]{:S(2)}) async-start(bf16[8,32,2048]{2,1,0:T(8,128)(2,1)} %bitcast.223), calls=%async_computation.1 | async-start | bytes 2097152 | tf_op jit(solution)/shard_map/all_to_all | solution.py:84
Sparse Core Ops, SparseCore 0:
  34.8 67.1 all-gather.11
  104.2 47.3 all-gather.7
  154.6 148.0 all-gather.9
where the time goes:
time: 364 us; the launch traced here: 363 us
  waiting for transfers between devices  251 us (69%)
  blocking collectives  53.4 us (15%)
  matrix products  15.7 us (4%)
  other arithmetic  14.3 us (4%)
  between operations  13.4 us (4%)
  starting transfers between devices  12.8 us (4%)
    all_gather x1, waiting for transfers between devices, in_one_piece(): whole = lax.all_gather(both, axis, axis=dim, tiled=True)  147 us
    all_gather x1, waiting for transfers between devices, gathered_once(): both, at, found = (lax.all_gather(jnp.concatenate(lines), axis), 0, {})  65.5 us
    all_to_all x2, blocking collectives, copy_for_each(): lax.all_to_all(jnp.broadcast_to(shard[None], (peers, *shard.shape)), axis...  42.6 us
    all_gather x1, waiting for transfers between devices, body(): full_out = lax.all_gather(emission_linear_map, 'tp', axis=0, tiled=True)  22.2 us
    all_to_all x1, waiting for transfers between devices, sum_at_owner(): lax.all_to_all(blocks, axis, split_axis=0, concat_axis=0, tiled=True)  15 us
    all_to_all x1, starting transfers between devices, sum_at_owner(): lax.all_to_all(blocks, axis, split_axis=0, concat_axis=0, tiled=True)  12.7 us
    all_gather x1, blocking collectives, gathered_once(): both, at, found = (lax.all_gather(jnp.concatenate(lines), axis), 0, {})  10.7 us
  transfers between devices with their start and end apart: 4, of which 4 were waited for; matrix products, arithmetic and copies ran while one was open for 2% of the time, Pallas kernels for 0%

commit v1 on v0

--- a/solution.py
+++ b/solution.py
@@ -184,7 +184,11 @@
     )
     mixed_heads = gated.reshape(positions, channels).astype(jnp.bfloat16)
     all_heads = gathered_copies(mixed_heads, "tp", 1)
-    full_out = lax.all_gather(emission_linear_map, "tp", axis=0, tiled=True)
+    rows = []
+    for _ in range(lax.axis_size("tp")):
+        rows.append(emission_linear_map)
+    v_next = jnp.concatenate(rows, axis=0)
+    full_out = lax.all_to_all(v_next, "tp", 0, 0, tiled=True)
     projected = jnp.dot(all_heads, full_out, preferred_element_type=jnp.float32)
     after_mix = residual_signal.astype(jnp.float32) + projected
     normed = (

time: 364 us -> 323 us (0.89)
  waiting for transfers between devices: 251 us -> 159 us
  blocking collectives: 53.4 us -> 82.4 us
  starting transfers between devices: 12.8 us -> 27.9 us
  local copies, waits for them, and re-layouts: 2.83 us -> 10.5 us
    all_gather x1, waiting for transfers between devices: 147 us -> 75.3 us  [in_one_piece(): whole = lax.all_gather(both, axis, axis=dim, tiled=True)]
    all_to_all x0 -> x1, blocking collectives: none -> 53.3 us  [body(): full_out = lax.all_to_all(v_next, 'tp', 0, 0, tiled=True)]
    all_to_all x2 -> x1, blocking collectives: 42.6 us -> 18.3 us  [copy_for_each(): lax.all_to_all(jnp.broadcast_to(shard[None], (peers, *shard.shape)), axis...]
    all_gather x1 -> x0, waiting for transfers between devices: 22.2 us -> none  [body(): full_out = lax.all_gather(emission_linear_map, 'tp', axis=0, tiled=True)]
    all_to_all x0 -> x1, starting transfers between devices: none -> 15.2 us  [copy_for_each(): lax.all_to_all(jnp.broadcast_to(shard[None], (peers, *shard.shape)), axis...]
    all_to_all x0 -> x1, waiting for transfers between devices: none -> 7.7 us  [copy_for_each(): lax.all_to_all(jnp.broadcast_to(shard[None], (peers, *shard.shape)), axis...]
    unnamed x17 -> x26, local copies, waits for them, and re-layouts: 2.1 us -> 7.96 us
    all_gather x1, waiting for transfers between devices: 65.5 us -> 61.3 us  [gathered_once(): both, at, found = (lax.all_gather(jnp.concatenate(lines), axis), 0, {})]
  transfers between devices with their start and end apart: 4 -> 4, of which waited for: 4 -> 4; matrix products, arithmetic and copies ran while one was open for 2% -> 4% of each run, Pallas kernels for 0% -> 0%
where the time goes in v1:
time: 323 us; the launch traced here: 322 us
  waiting for transfers between devices  159 us (49%)
  blocking collectives  82.4 us (26%)
  starting transfers between devices  27.9 us (9%)
  other arithmetic  15.1 us (5%)
  between operations  13.7 us (4%)
  matrix products  13.3 us (4%)
  local copies, waits for them, and re-layouts  10.5 us (3%)
    all_gather x1, waiting for transfers between devices, in_one_piece(): whole = lax.all_gather(both, axis, axis=dim, tiled=True)  75.3 us
    all_gather x1, waiting for transfers between devices, gathered_once(): both, at, found = (lax.all_gather(jnp.concatenate(lines), axis), 0, {})  61.3 us
    all_to_all x1, blocking collectives, body(): full_out = lax.all_to_all(v_next, 'tp', 0, 0, tiled=True)  53.3 us
    all_to_all x1, blocking collectives, copy_for_each(): lax.all_to_all(jnp.broadcast_to(shard[None], (peers, *shard.shape)), axis...  18.3 us
    all_to_all x1, starting transfers between devices, copy_for_each(): lax.all_to_all(jnp.broadcast_to(shard[None], (peers, *shard.shape)), axis...  15.2 us
    all_to_all x1, waiting for transfers between devices, sum_at_owner(): lax.all_to_all(blocks, axis, split_axis=0, concat_axis=0, tiled=True)  15 us
    all_to_all x1, starting transfers between devices, sum_at_owner(): lax.all_to_all(blocks, axis, split_axis=0, concat_axis=0, tiled=True)  12.7 us
    all_gather x1, blocking collectives, gathered_once(): both, at, found = (lax.all_gather(jnp.concatenate(lines), axis), 0, {})  10.7 us
  transfers between devices with their start and end apart: 4, of which 4 were waited for; matrix products, arithmetic and copies ran while one was open for 4% of the time, Pallas kernels for 0%

profile of v1, /device:TPU:1, one launch (start us, length us, event | category | flops | bytes accessed | tf_op | source)
XLA Modules:
  0.0 322.4 jit_solution(15501872382240275079)
XLA Ops:
  7.2 1.1 exponential-minus-one_negate_fusion
  8.8 1.0 copy.43
  10.0 0.9 convert.1
  10.9 13.1 %while.13 = (s32[]{:T(128)}, f32[1,128,128]{2,1,0:T(8,128)S(1)}, f32[4,1,64,128]{3,2,1,0:T(8,128)S(1)}, f32[4,1,64,128]{3,2,1,0:T(8,128)S(1)}, f32[4,1,64,128]{3...) while((s32[]{:T(128)}, f32[1,128,128]{2,1,0:T(8,128)S(1)}, ...), condition=%wide.region_2.3_spmd.clone, body=%wide.region_0.2_spmd.clone.sunk | while | flops 34693120 | bytes 5108864 | solution.py:153
  11.7 1.7 fusion.175
  14.9 1.7 fusion.175
  18.2 1.7 fusion.175
  21.5 1.7 fusion.175
  24.0 10.7 %all-gather.2 = f32[4,129,128]{2,1,0:T(8,128)S(1)} all-gather(f32[1,129,128]{2,1,0:T(8,128)S(1)} %maximum_bitcast_fusion), channel_id=2, replica_groups=mesh['sp_0'=16,'sp_1'=4,'tp'=8] {'sp_1'}, dimensions={0}, use_global_device_ids=true | all-gather | bytes 330240 | tf_op jit(solution)/shard_map/all_gather | solution.py:28
  36.6 0.9 constant_dynamic-update-slice_fusion.7
  37.4 0.9 constant_dynamic-update-slice_fusion.6
  41.6 61.3 %all-gather.9.cloned.1.call-done = f32[16,129,128]{2,1,0:T(8,128)} async-done(((f32[1,129,128]{2,1,0:T(8,128)}), f32[16,129,128]{2,1,0:T(8,128)}) %all-gather.9.cloned.1.call-update) | async-done | bytes 1056784 | tf_op jit(solution)/shard_map/all_gather | solution.py:28
  103.6 2.1 multiply_reduce_fusion.1
  106.0 0.9 broadcast_in_dim.32
  106.8 15.2 %all-to-all-start = ((bf16[8,256,128]{2,1,0:T(8,128)(2,1)}), bf16[8,256,128]{2,1,0:T(8,128)(2,1)S(1)}, u32[]{:S(2)}, u32[]{:S(2)}) async-start(bf16[8,256,128]{2,1,0:T(8,128)(2,1)} %broadcast_in_dim.32), calls=%async_computation | async-start | bytes 1048576 | tf_op jit(solution)/shard_map/all_to_all | solution.py:60
  123.7 7.7 %all-to-all-done = bf16[8,256,128]{2,1,0:T(8,128)(2,1)S(1)} async-done(((bf16[8,256,128]{2,1,0:T(8,128)(2,1)}), bf16[8,256,128]{2,1,0:T(8,128)(2,1)S(1)}, u32[]{:S(2)}, u32[]{:S(2)}) %all-to-all-start) | async-done | bytes 524320 | tf_op jit(solution)/shard_map/all_to_all | solution.py:60
  131.4 53.3 %all_to_all.24 = bf16[8,128,2048]{2,1,0:T(8,128)(2,1)S(1)} all-to-all(bf16[8,128,2048]{2,1,0:T(8,128)(2,1)} %bitcast.42), channel_id=1, replica_groups=mesh['sp_0'=16,'sp_1'=4,'tp'=8] {'tp'}, dimensions={0} | all-to-all | bytes 8388608 | tf_op jit(solution)/shard_map/all_to_all | solution.py:191
  184.7 1.5 multiply_reduce_fusion
  186.2 75.3 %all-gather.7.cloned.1.call-done = bf16[2048,2048]{1,0:T(8,128)(2,1)} async-done(((bf16[32,2048]{1,0:T(8,128)(2,1)}), bf16[2048,2048]{1,0:T(8,128)(2,1)}) %all-gather.7.cloned.1.call-update) | async-done | bytes 8388624 | tf_op jit(solution)/shard_map/all_gather | solution.py:72
  261.5 6.8 %fusion.33 = bf16[256,2048]{1,0:T(8,128)(2,1)} fusion(bf16[2048,2048]{1,0:T(8,128)(2,1)} %all-gather.7.cloned.1.call-done, f32[256,2048]{1,0:T(8,128)S(1)} %get-tuple-element.142, f32[2048]{0:T(1024)S(1)} %copy-done.6, f32[256]{0:T(256)S(1)} %add_rsqrt_fusion), kind=kOutput, calls=%fused_computation.43 | convolution fusion | flops 2150367232 | bytes 11543552 | tf_op jit(solution)/shard_map/dot_general | solution.py:204
  268.3 12.7 %all-to-all-start.2 = ((bf16[8,32,2048]{2,1,0:T(8,128)(2,1)}), bf16[8,32,2048]{2,1,0:T(8,128)(2,1)S(1)}, u32[]{:S(2)}, u32[]{:S(2)}) async-start(bf16[8,32,2048]{2,1,0:T(8,128)(2,1)} %bitcast.44), calls=%async_computation.2 | async-start | bytes 2097152 | tf_op jit(solution)/shard_map/all_to_all | solution.py:84
  281.0 15.0 %all-to-all-done.2 = bf16[8,32,2048]{2,1,0:T(8,128)(2,1)S(1)} async-done(((bf16[8,32,2048]{2,1,0:T(8,128)(2,1)}), bf16[8,32,2048]{2,1,0:T(8,128)(2,1)S(1)}, u32[]{:S(2)}, u32[]{:S(2)}) %all-to-all-start.2) | async-done | bytes 1048608 | tf_op jit(solution)/shard_map/all_to_all | solution.py:84
  296.3 18.3 %all_to_all.25 = bf16[8,32,2048]{2,1,0:T(8,128)(2,1)S(1)} all-to-all(bf16[8,32,2048]{2,1,0:T(8,128)(2,1)S(1)} %broadcast_in_dim.33), channel_id=1, replica_groups=mesh['sp_0'=16,'sp_1'=4,'tp'=8] {'tp'}, dimensions={0} | all-to-all | bytes 2097152 | tf_op jit(solution)/shard_map/all_to_all | solution.py:60
  314.6 1.0 copy.90
  (96 shorter events, 15.2 us)
Async XLA Ops:
  6.5 96.3 %all-gather.9.cloned.1.call-start = ((), (), s32[]{:S(2)}) async-start(), calls=%async_computation.5 | async-start | bytes 1183744 | tf_op jit(solution)/shard_map/all_gather | solution.py:28
  10.8 24.7 %copy-start.2 = (bf16[32,1024]{1,0:T(8,128)(2,1)S(1)}, bf16[32,1024]{1,0:T(8,128)(2,1)}, u32[]{:S(2)}) copy-start(bf16[32,1024]{1,0:T(8,128)(2,1)} %param.25) | copy-start | bytes 196612
  10.8 24.7 %copy-start.3 = (bf16[32,1024]{1,0:T(8,128)(2,1)S(1)}, bf16[32,1024]{1,0:T(8,128)(2,1)}, u32[]{:S(2)}) copy-start(bf16[32,1024]{1,0:T(8,128)(2,1)} %param.24) | copy-start | bytes 196612
  10.9 25.6 %copy-start.1 = (bf16[256,128]{1,0:T(8,128)(2,1)S(1)}, bf16[256,128]{1,0:T(8,128)(2,1)}, u32[]{:S(2)}) copy-start(bf16[256,128]{1,0:T(8,128)(2,1)} %param.18) | copy-start | bytes 196612
  10.9 25.7 %copy-start = (bf16[128,2048]{1,0:T(8,128)(2,1)S(1)}, bf16[128,2048]{1,0:T(8,128)(2,1)}, u32[]{:S(2)}) copy-start(bf16[128,2048]{1,0:T(8,128)(2,1)} %param.22) | copy-start | bytes 1572868
  35.5 226.0 %all-gather.7.cloned.1.call-start = ((), (), s32[]{:S(2)}) async-start(), calls=%async_computation.4 | async-start | bytes 8519680 | tf_op jit(solution)/shard_map/all_gather | solution.py:72
  37.4 68.3 %copy-start.4 = (f32[128]{0:T(128)S(1)}, f32[128]{0:T(128)}, u32[]{:S(2)}) copy-start(f32[128]{0:T(128)} %param.21) | copy-start | bytes 1540
  106.8 24.5 %all-to-all-start = ((bf16[8,256,128]{2,1,0:T(8,128)(2,1)}), bf16[8,256,128]{2,1,0:T(8,128)(2,1)S(1)}, u32[]{:S(2)}, u32[]{:S(2)}) async-start(bf16[8,256,128]{2,1,0:T(8,128)(2,1)} %broadcast_in_dim.32), calls=%async_computation | async-start | bytes 1048576 | tf_op jit(solution)/shard_map/all_to_all | solution.py:60
  131.4 53.3 %copy-start.5 = (bf16[256,2048]{1,0:T(8,128)(2,1)S(1)}, bf16[256,2048]{1,0:T(8,128)(2,1)}, u32[]{:S(2)}) copy-start(bf16[256,2048]{1,0:T(8,128)(2,1)} %param.14) | copy-start | bytes 3145732
  184.7 76.7 %copy-start.6 = (f32[2048]{0:T(1024)S(1)}, f32[2048]{0:T(1024)}, u32[]{:S(2)}) copy-start(f32[2048]{0:T(1024)} %param.23) | copy-start | bytes 24580
  268.3 27.6 %all-to-all-start.2 = ((bf16[8,32,2048]{2,1,0:T(8,128)(2,1)}), bf16[8,32,2048]{2,1,0:T(8,128)(2,1)S(1)}, u32[]{:S(2)}, u32[]{:S(2)}) async-start(bf16[8,32,2048]{2,1,0:T(8,128)(2,1)} %bitcast.44), calls=%async_computation.2 | async-start | bytes 2097152 | tf_op jit(solution)/shard_map/all_to_all | solution.py:84
Sparse Core Ops, SparseCore 0:
  35.6 67.1 all-gather.8
  105.8 155.6 all-gather.6
